TPU v7x, 32 devices: a whole 2x2x4 slice. The times are simulated.
32 devices in a mesh: ep: 8 (over z, x), tp: 4 (over y, core).
Axes of the slice: x: 2, y: 2, z: 4, core: 2. Of those that a mesh axis runs over, the one named last changes fastest.
Arguments:
- hidden_in: bfloat16 [128, 4096], P('ep'), may hold values from -6 to 6
- w_query: bfloat16 [4096, 2048], P('ep', 'tp'), may hold values from -0.09375 to 0.09375
- w_key: bfloat16 [4096, 2048], P('ep', 'tp'), may hold values from -0.09375 to 0.09375
- w_value: bfloat16 [4096, 2048], P('ep', 'tp'), may hold values from -0.09375 to 0.09375
- w_outgate: bfloat16 [4096, 2048], P('ep', 'tp'), may hold values from -0.09375 to 0.09375
- w_igate: bfloat16 [4096, 16], P('ep', 'tp'), may hold values from -0.09375 to 0.09375
- w_fgate: bfloat16 [4096, 16], P('ep', 'tp'), may hold values from -0.09375 to 0.09375
- input_bias: float32 [16], P('tp'), may hold values from -3 to 303
- forget_bias: float32 [16], P('tp'), may hold values from -1 to 5
- mem_state: float32 [128, 16, 16384], P('ep', 'tp'), may hold values from -4 to 4
- max_state: float32 [128, 16], P('ep', 'tp'), may hold values from -4 to 304
- head_gain: float32 [2048], P('tp'), may hold values from 0.1 to 1.9
- w_output: bfloat16 [2048, 4096], P('tp'), may hold values from -0.26367188 to 0.26367188
- first_gain: float32 [4096], replicated, may hold values from 0.35 to 3.25
- w_group_router: bfloat16 [4096, 2], replicated, may hold values from -0.09375 to 0.09375
- w_expert_router: bfloat16 [4096, 8], replicated, may hold values from -0.09375 to 0.09375
- expert_route: int32 [128, 2], P('ep'), may hold values from 0 to 7, as said below
- w_expgate: bfloat16 [8, 4096, 1024], P('ep', None, 'tp'), may hold values from -0.09375 to 0.09375
- w_expup: bfloat16 [8, 4096, 1024], P('ep', None, 'tp'), may hold values from -0.09375 to 0.09375
- w_expdown: bfloat16 [8, 1024, 4096], P('ep', 'tp'), may hold values from -0.75 to 0.75
- second_gain: float32 [4096], P('tp'), may hold values from 0.1 to 1.9
Outputs:
- hidden_out: bfloat16 [128, 4096], P('ep', 'tp')
- mem_next: float32 [128, 16, 16384], P('ep', 'tp')
- max_next: float32 [128, 16], P('ep', 'tp')
Inputs may be any that keep to these rules, and one draw needn't show every extreme that they name: `expert_route`: each row names two different experts of one group (an expert's group is its number divided by 4). In each aligned block of 16 rows (the rows of one index of ep) every group is named by exactly 8 rows, no expert by more than 8 rows, and some expert by exactly 8 rows.
All inputs are finite; a program needn't handle non-finite values.
Results may differ from a plain program's by a relative error of at most 0.02.
Values may be sent and summed in bfloat16 or wider, within the bound.
No kernel may reach another device: no remote copies, remote signals or barrier semaphores. Data moves between devices by JAX's collectives and lax.ppermute only.
A program may use at most 64 MiB of HBM per device.

v0:
```python
import jax
import jax.numpy as jnp
from jax import lax
from jax.sharding import PartitionSpec as P

D = 4096
DH = 128
GROUP_SIZE = 4


res_alpha = 8.0**0.25


def layer_norm(values, gain):
    row_mean = jnp.mean(values, -1, keepdims=True)
    row_var = jnp.mean(values * values, -1, keepdims=True) - row_mean * row_mean
    return (values - row_mean) * lax.rsqrt(row_var + 1e-05) * gain


def mlstm_step(queries, keys_scaled, values, log_input, log_forget, memory, stabilizer):
    new_max = jnp.maximum(log_forget + stabilizer, log_input)
    keep_old = jnp.exp(log_forget + stabilizer - new_max)
    write_new = jnp.exp(log_input - new_max)
    scores = jnp.sum(queries * keys_scaled, -1) * write_new
    read_old = jnp.einsum("bhd,bhde->bhe", queries, memory, precision=lax.Precision.HIGHEST)
    readout = scores[..., None] * values + keep_old[..., None] * read_old
    memory_next = (
        keep_old[..., None, None] * memory
        + write_new[..., None, None] * keys_scaled[..., :, None] * values[..., None, :]
    )
    return (readout, memory_next, new_max)


def head_mix(readout, head_gain, out_pre):
    scaled = readout * lax.rsqrt(jnp.mean(readout * readout, -1, keepdims=True) + 1e-06)
    flat_heads = scaled.reshape(scaled.shape[0], -1)
    return (flat_heads * head_gain * jax.nn.sigmoid(out_pre)).astype(jnp.bfloat16)


def route_weights(mid_float, w_group_router, w_expert_router, expert_route):
    group_logits = jnp.dot(
        mid_float, w_group_router.astype(jnp.float32), precision=lax.Precision.HIGHEST
    )
    expert_logits = jnp.dot(
        mid_float, w_expert_router.astype(jnp.float32), precision=lax.Precision.HIGHEST
    )
    first_expert = expert_route[:, 0]
    second_expert = expert_route[:, 1]
    expert_ids = lax.broadcasted_iota(jnp.int32, expert_logits.shape, 1)
    group_ids = lax.broadcasted_iota(jnp.int32, group_logits.shape, 1)
    first_logit = jnp.sum(jnp.where(expert_ids == first_expert[:, None], expert_logits, 0.0), -1)
    second_logit = jnp.sum(jnp.where(expert_ids == second_expert[:, None], expert_logits, 0.0), -1)
    group_pick = jnp.sum(
        jnp.where(group_ids == (first_expert // GROUP_SIZE)[:, None], group_logits, 0.0), -1
    )
    group_gate = jax.nn.sigmoid(group_pick)
    return (
        group_gate * jax.nn.sigmoid(first_logit - second_logit),
        group_gate * jax.nn.sigmoid(second_logit - first_logit),
    )


def slot_ranks(flat_routes, expert_total):
    onehot = (
        flat_routes[:, None]
        == lax.broadcasted_iota(jnp.int32, (flat_routes.shape[0], expert_total), 1)
    ).astype(jnp.int32)
    running = jnp.cumsum(onehot, 0)
    return jnp.sum((running - 1) * onehot, -1)


def body(
    hidden_in,
    w_query,
    w_key,
    w_value,
    w_outgate,
    w_igate,
    w_fgate,
    input_bias,
    forget_bias,
    mem_state,
    max_state,
    head_gain,
    w_output,
    first_gain,
    w_group_router,
    w_expert_router,
    expert_route,
    w_expgate,
    w_expup,
    w_expdown,
    second_gain,
):
    own_rows, width = hidden_in.shape
    heads_here = mem_state.shape[1]
    head_width = heads_here * DH
    top_count = expert_route.shape[1]
    spread_rows = lax.all_to_all(hidden_in, "ep", split_axis=1, concat_axis=0, tiled=True)
    stacked_w = jnp.concatenate([w_query, w_key, w_value, w_outgate], 1)
    gate_w = jnp.concatenate([w_igate, w_fgate], 1)
    proj_terms = jnp.dot(spread_rows, stacked_w, preferred_element_type=jnp.float32)
    gate_terms = jnp.dot(spread_rows, gate_w, preferred_element_type=jnp.float32)
    projected, gate_sums = (
        lax.psum_scatter(proj_terms, "ep", scatter_dimension=0, tiled=True),
        lax.psum_scatter(gate_terms, "ep", scatter_dimension=0, tiled=True),
    )
    shaped = projected.reshape(own_rows, 4, heads_here, DH)
    queries = shaped[:, 0]
    keys_raw = shaped[:, 1]
    values = shaped[:, 2]
    out_pre = shaped[:, 3].reshape(own_rows, head_width)
    input_sum = gate_sums[:, :heads_here]
    forget_sum = gate_sums[:, heads_here:]
    keys_scaled = keys_raw * DH ** (-0.5)
    log_input = input_sum + input_bias
    log_forget = jax.nn.log_sigmoid(forget_sum + forget_bias)
    memory = mem_state.reshape(own_rows, heads_here, DH, DH)
    readout, memory_square, new_max = mlstm_step(
        queries, keys_scaled, values, log_input, log_forget, memory, max_state
    )
    memory_next = memory_square.reshape(own_rows, heads_here, DH * DH)
    mixed_heads = head_mix(readout, head_gain, out_pre)
    partial_mix = jnp.dot(mixed_heads, w_output, preferred_element_type=jnp.float32).astype(
        jnp.bfloat16
    )
    mix = lax.psum(partial_mix.astype(jnp.float32).astype(jnp.bfloat16), "tp").astype(jnp.float32)
    mid_float = layer_norm(res_alpha * hidden_in.astype(jnp.float32) + mix, first_gain)
    mid = mid_float.astype(jnp.bfloat16)
    first_weight, second_weight = route_weights(
        mid_float, w_group_router, w_expert_router, expert_route
    )
    expert_total = w_expgate.shape[0] * lax.axis_size("ep")
    capacity = 2 * own_rows * top_count // expert_total
    flat_routes = expert_route.reshape(-1)
    local_slot = flat_routes * capacity + slot_ranks(flat_routes, expert_total)
    share_width = width // lax.axis_size("tp")
    mid_share = lax.dynamic_slice_in_dim(mid, lax.axis_index("tp") * share_width, share_width, 1)
    buffer = (
        jnp.zeros((expert_total * capacity, width), jnp.bfloat16)
        .at[local_slot]
        .set(jnp.repeat(mid, top_count, 0))
    )
    arrived = lax.all_to_all(
        buffer.reshape(expert_total, capacity, width), "ep", split_axis=0, concat_axis=1, tiled=True
    )
    gate_pre = jnp.einsum("erd,edf->erf", arrived, w_expgate, preferred_element_type=jnp.float32)
    up_pre = jnp.einsum("erd,edf->erf", arrived, w_expup, preferred_element_type=jnp.float32)
    hidden_units = (jax.nn.silu(gate_pre) * up_pre).astype(jnp.bfloat16)
    down_terms = jnp.einsum(
        "erf,efd->erd", hidden_units, w_expdown, preferred_element_type=jnp.float32
    ).astype(jnp.bfloat16)
    expert_share = lax.psum_scatter(
        down_terms.astype(jnp.float32).astype(jnp.bfloat16), "tp", scatter_dimension=2, tiled=True
    )
    returned = lax.all_to_all(expert_share, "ep", split_axis=1, concat_axis=0, tiled=True)
    picked = returned.reshape(expert_total * capacity, share_width)[local_slot]
    picked = picked.astype(jnp.float32).reshape(own_rows, top_count, share_width)
    moe = first_weight[:, None] * picked[:, 0] + second_weight[:, None] * picked[:, 1]
    joined = res_alpha * mid_share.astype(jnp.float32) + moe
    row_sum, square_sum = lax.psum((jnp.sum(joined, -1), jnp.sum(joined * joined, -1)), "tp")
    row_mean = row_sum / D
    row_var = square_sum / D - row_mean * row_mean
    hidden_out = (
        (joined - row_mean[:, None]) * lax.rsqrt(row_var[:, None] + 1e-05) * second_gain
    ).astype(jnp.bfloat16)
    return (hidden_out, memory_next, new_max)


def solution(mesh):
    return jax.shard_map(
        body,
        mesh=mesh,
        in_specs=(
            P("ep", None),
            P("ep", "tp"),
            P("ep", "tp"),
            P("ep", "tp"),
            P("ep", "tp"),
            P("ep", "tp"),
            P("ep", "tp"),
            P("tp"),
            P("tp"),
            P("ep", "tp", None),
            P("ep", "tp"),
            P("tp"),
            P("tp", None),
            P(),
            P(),
            P(),
            P("ep", None),
            P("ep", None, "tp"),
            P("ep", None, "tp"),
            P("ep", "tp", None),
            P("tp"),
        ),
        out_specs=(P("ep", "tp"), P("ep", "tp", None), P("ep", "tp")),
        check_vma=False,
    )
```

profile of v0, /device:TPU:0, one launch (start us, length us, event | category | flops | bytes accessed | tf_op | source)
XLA Modules:
  0.0 277.9 jit_solution(14590576950777728029)
XLA Ops:
  7.2 1.1 copy.139
  8.3 14.4 %all_to_all.37 = bf16[16,8,512]{2,0,1:T(8,128)(2,1)S(1)} all-to-all(bf16[16,8,512]{2,0,1:T(8,128)(2,1)S(1)} %bitcast.124), channel_id=1, replica_groups=mesh['ep'=8,'tp'=4] {'ep'}, dimensions={1} | all-to-all | bytes 262144 | tf_op jit(solution)/shard_map/all_to_all | solution.py:99
  24.4 2.3 convolution_bitcast_fusion
  26.6 1.3 copy.104
  28.1 6.1 %reshape.183 = f32[16,4,128,128]{3,2,1,0:T(8,128)} reshape(f32[16,4,16384]{2,1,0:T(4,128)} %param.30) | data formatting | bytes 8388608 | tf_op jit(solution)/shard_map/reshape | solution.py:118
  34.9 49.9 %reduce-scatter.12.cloned.1.call-done = f32[16,8]{1,0:T(8,128)} async-done(((f32[128,8]{1,0:T(8,128)}), f32[16,8]{1,0:T(8,128)}) %reduce-scatter.12.cloned.1.call-update) | async-done | bytes 528 | tf_op jit(solution)/shard_map/reduce_scatter | solution.py:106
  84.8 0.9 broadcast_multiply_fusion.2
  85.7 66.2 %reduce-scatter.10.cloned.1.call-done = f32[16,2048]{1,0:T(8,128)} async-done(((f32[128,2048]{1,0:T(8,128)}), f32[16,2048]{1,0:T(8,128)}) %reduce-scatter.10.cloned.1.call-update) | async-done | bytes 131088
  151.8 1.2 copy.105
  153.1 0.9 fusion.62
  154.0 1.0 copy.109
  155.1 1.1 copy.110
  156.1 1.1 copy.111
  157.3 5.3 %fusion.64 = f32[16,4,1,128]{3,2,1,0:T(1,128)S(1)} fusion(f32[16,4,128,1]{2,3,1,0:T(1,128)S(1)} %bitcast.125, f32[16,4,128,128]{3,2,1,0:T(8,128)} %reshape.183), kind=kOutput, calls=%fused_computation.111 | convolution fusion | flops 12582912 | bytes 4259840 | tf_op jit(solution)/shard_map/bhd,bhde->bhe/dot_general | solution.py:25
  163.3 3.5 %convolution_convert_fusion.1 = bf16[16,4096]{1,0:T(8,128)(2,1)} fusion(bf16[512,4096]{1,0:T(8,128)(2,1)} %param.33, f32[2,8,4,128]{3,2,1,0:T(4,128)S(1)} %bitcast.128, f32[2,8,4,128]{3,2,1,0:T(4,128)S(1)} %bitcast.129, f32[512]{0:T(512)S(1)} %copy-done.7), kind=kOutput, calls=%fused_computation.4 | convolution fusion | flops 67198976 | bytes 4392960 | tf_op jit(solution)/shard_map/dot_general | solution.py:124
  166.8 30.9 %all-reduce.3.cloned.1.call-done = bf16[16,4096]{1,0:T(8,128)(2,1)} async-done(((bf16[16,4096]{1,0:T(8,128)(2,1)}), bf16[16,4096]{1,0:T(8,128)(2,1)}) %all-reduce.3.cloned.1.call-update) | async-done | bytes 131088 | tf_op jit(solution)/shard_map/psum | solution.py:127
  197.7 1.1 fusion.27
  198.8 1.0 fusion.58
  200.1 1.8 scatter_custom_fusion
  201.9 5.5 %all-to-all-start.1 = ((bf16[8,8,4096]{2,1,0:T(8,128)(2,1)}), bf16[8,8,4096]{2,1,0:T(8,128)(2,1)S(1)}, u32[]{:S(2)}, u32[]{:S(2)}) async-start(bf16[8,8,4096]{2,1,0:T(8,128)(2,1)} %bitcast.18), calls=%async_computation.1 | async-start | bytes 1048576 | tf_op jit(solution)/shard_map/all_to_all | solution.py:144
  208.1 2.6 broadcast_multiply_fusion
  210.8 5.6 %mul.268 = f32[16,4,16384]{2,1,0:T(4,128)} reshape(f32[16,4,128,128]{3,2,1,0:T(8,128)} %broadcast_multiply_fusion) | data formatting | bytes 8388608 | tf_op jit(solution)/shard_map/mul | solution.py:29
  216.3 4.5 %all-to-all-done.1 = bf16[8,8,4096]{2,1,0:T(8,128)(2,1)S(1)} async-done(((bf16[8,8,4096]{2,1,0:T(8,128)(2,1)}), bf16[8,8,4096]{2,1,0:T(8,128)(2,1)S(1)}, u32[]{:S(2)}, u32[]{:S(2)}) %all-to-all-start.1) | async-done | bytes 524320 | tf_op jit(solution)/shard_map/all_to_all | solution.py:144
  220.8 2.0 fusion.11
  222.9 3.8 %fusion = bf16[1,64,4096]{2,1,0:T(8,128)(2,1)} fusion(bf16[1,256,4096]{2,1,0:T(8,128)(2,1)S(1)} %copy-done, bf16[1,4096,256]{2,1,0:T(8,128)(2,1)} %param.39, bf16[8,8,4096]{2,1,0:T(8,128)(2,1)S(1)} %all-to-all-done.1, f32[64,256]{1,0:T(8,128)S(1)} %fusion.11), kind=kOutput, calls=%fused_computation.3 | convolution fusion | flops 268795904 | bytes 5308416 | tf_op jit(solution)/shard_map/erf,efd->erd/dot_general | solution.py:150
  226.7 6.9 %multiply_add_fusion = f32[16,4,16384]{2,1,0:T(4,128)} fusion(f32[16,4,16384]{2,1,0:T(4,128)} %mul.268, f32[16,4,16384]{2,1,0:T(4,128)} %param.30, f32[16,4]{1,0:T(8,128)S(1)} %get-tuple-element.28), kind=kLoop, calls=%fused_computation.5 | loop fusion | flops 2097152 | bytes 12583168 | tf_op jit(solution)/shard_map/add | solution.py:28
  234.4 12.5 %reduce-scatter.8.cloned.1.call-done = bf16[1,64,1024]{2,1,0:T(8,128)(2,1)} async-done(((bf16[1,64,4096]{2,1,0:T(8,128)(2,1)}), bf16[1,64,1024]{2,1,0:T(8,128)(2,1)}) %reduce-scatter.8.cloned.1.call-update) | async-done | bytes 131088 | tf_op jit(solution)/shard_map/reduce_scatter | solution.py:153
  246.9 1.1 copy.141
  248.5 1.4 reduce
  250.6 5.5 %all-to-all-start.2 = ((bf16[8,2,4096]{2,1,0:T(2,128)(2,1)}), bf16[8,2,4096]{2,1,0:T(2,128)(2,1)S(1)}, u32[]{:S(2)}, u32[]{:S(2)}) async-start(bf16[8,2,4096]{2,1,0:T(2,128)(2,1)} %reshape.217), calls=%async_computation.3 | async-start | bytes 262144 | tf_op jit(solution)/shard_map/all_to_all | solution.py:156
  256.2 7.3 %all-to-all-done.2 = bf16[8,2,4096]{2,1,0:T(2,128)(2,1)S(1)} async-done(((bf16[8,2,4096]{2,1,0:T(2,128)(2,1)}), bf16[8,2,4096]{2,1,0:T(2,128)(2,1)S(1)}, u32[]{:S(2)}, u32[]{:S(2)}) %all-to-all-start.2) | async-done | bytes 131104 | tf_op jit(solution)/shard_map/all_to_all | solution.py:156
  264.7 5.9 %all-reduce = (f32[16]{0:T(128)S(1)}, f32[16]{0:T(128)S(1)}) all-reduce(f32[16]{0:T(128)S(1)} %get-tuple-element.9, f32[16]{0:T(128)S(1)} %get-tuple-element.8), channel_id=1, replica_groups=mesh['ep'=8,'tp'=4] {'tp'}, use_global_device_ids=true, to_apply=%region_17.18 | all-reduce | flops 32 | bytes 256 | tf_op jit(solution)/shard_map/psum | solution.py:161
  (74 shorter events, 8.2 us)
Async XLA Ops:
  7.2 215.7 %copy-start = (bf16[1,256,4096]{2,1,0:T(8,128)(2,1)S(1)}, bf16[1,256,4096]{2,1,0:T(8,128)(2,1)}, u32[]{:S(2)}) copy-start(bf16[1,256,4096]{2,1,0:T(8,128)(2,1)} %param.40) | copy-start | bytes 6291460
  7.2 77.6 %reduce-scatter.12.cloned.1.call-start = ((), (), s32[]{:S(2)}) async-start(), calls=%async_computation.9 | async-start | bytes 73728 | tf_op jit(solution)/shard_map/reduce_scatter | solution.py:106
  24.3 3.7 %copy-start.10 = (f32[16,4]{0,1:T(4,128)S(1)}, f32[16,4]{0,1:T(4,128)}, u32[]{:S(2)}) copy-start(f32[16,4]{0,1:T(4,128)} %param.31) | copy-start | bytes 772
  24.3 127.5 %reduce-scatter.10.cloned.1.call-start = ((), (), s32[]{:S(2)}) async-start(), calls=%async_computation.8 | async-start | bytes 1179648
  28.0 169.7 %all-reduce.3.cloned.1.call-start = ((), (), s32[]{:S(2)}) async-start(), calls=%async_computation.6 | async-start | bytes 262144 | tf_op jit(solution)/shard_map/psum | solution.py:127
  28.1 6.1 %copy-start.5 = (s32[16,2]{0,1:T(2,128)S(1)}, s32[16,2]{0,1:T(2,128)}, u32[]{:S(2)}) copy-start(s32[16,2]{0,1:T(2,128)} %param.37) | copy-start | bytes 388
  28.1 56.7 %copy-start.8 = (f32[4]{0:T(128)S(1)}, f32[4]{0:T(128)}, u32[]{:S(2)}) copy-start(f32[4]{0:T(128)} %param.28) | copy-start | bytes 52
  28.1 56.7 %copy-start.9 = (f32[4]{0:T(128)S(1)}, f32[4]{0:T(128)}, u32[]{:S(2)}) copy-start(f32[4]{0:T(128)} %param.29) | copy-start | bytes 52
  85.7 77.0 %copy-start.3 = (f32[16,8]{1,0:T(8,128)S(1)}, f32[16,8]{1,0:T(8,128)}, u32[]{:S(2)}) copy-start(f32[16,8]{1,0:T(8,128)} %reduce-scatter.12.cloned.1.call-done) | copy-start | bytes 1540
  153.1 10.2 %copy-start.7 = (f32[512]{0:T(512)S(1)}, f32[512]{0:T(512)}, u32[]{:S(2)}) copy-start(f32[512]{0:T(512)} %param.32) | copy-start | bytes 6148
  157.3 40.4 %copy-start.1 = (bf16[16,4096]{1,0:T(8,128)(2,1)S(1)}, bf16[16,4096]{1,0:T(8,128)(2,1)}, u32[]{:S(2)}) copy-start(bf16[16,4096]{1,0:T(8,128)(2,1)} %param.21) | copy-start | bytes 393220
  157.3 41.5 %copy-start.4 = (f32[4096]{0:T(1024)S(1)}, f32[4096]{0:T(1024)}, u32[]{:S(2)}) copy-start(f32[4096]{0:T(1024)} %param.34) | copy-start | bytes 49156
  201.9 18.9 %all-to-all-start.1 = ((bf16[8,8,4096]{2,1,0:T(8,128)(2,1)}), bf16[8,8,4096]{2,1,0:T(8,128)(2,1)S(1)}, u32[]{:S(2)}, u32[]{:S(2)}) async-start(bf16[8,8,4096]{2,1,0:T(8,128)(2,1)} %bitcast.18), calls=%async_computation.1 | async-start | bytes 1048576 | tf_op jit(solution)/shard_map/all_to_all | solution.py:144
  207.4 39.5 %reduce-scatter.8.cloned.1.call-start = ((), (), s32[]{:S(2)}) async-start(), calls=%async_computation.7 | async-start | bytes 655360 | tf_op jit(solution)/shard_map/reduce_scatter | solution.py:153
  226.7 6.9 %copy-start.2 = (bf16[16,4096]{1,0:T(8,128)(2,1)S(1)}, bf16[16,4096]{1,0:T(8,128)(2,1)}, u32[]{:S(2)}) copy-start(bf16[16,4096]{1,0:T(8,128)(2,1)} %all-reduce.3.cloned.1.call-done) | copy-start | bytes 393220
  226.7 6.9 %copy-start.12 = (bf16[4096,2]{0,1:T(2,128)(2,1)S(1)}, bf16[4096,2]{0,1:T(2,128)(2,1)}, u32[]{:S(2)}) copy-start(bf16[4096,2]{0,1:T(2,128)(2,1)} %param.35) | copy-start | bytes 49156
  226.7 7.3 %copy-start.11 = (bf16[4096,8]{0,1:T(8,128)(2,1)S(1)}, bf16[4096,8]{0,1:T(8,128)(2,1)}, u32[]{:S(2)}) copy-start(bf16[4096,8]{0,1:T(8,128)(2,1)} %param.36) | copy-start | bytes 196612
  233.6 37.1 %copy-start.6 = (f32[1024]{0:T(1024)S(1)}, f32[1024]{0:T(1024)}, u32[]{:S(2)}) copy-start(f32[1024]{0:T(1024)} %param.41) | copy-start | bytes 12292
  250.6 12.9 %all-to-all-start.2 = ((bf16[8,2,4096]{2,1,0:T(2,128)(2,1)}), bf16[8,2,4096]{2,1,0:T(2,128)(2,1)S(1)}, u32[]{:S(2)}, u32[]{:S(2)}) async-start(bf16[8,2,4096]{2,1,0:T(2,128)(2,1)} %reshape.217), calls=%async_computation.3 | async-start | bytes 262144 | tf_op jit(solution)/shard_map/all_to_all | solution.py:156
Sparse Core Ops, SparseCore 0:
  24.4 60.3 reduce-scatter.11
  88.2 63.5 reduce-scatter.9
  166.9 30.7 all-reduce.2
  226.8 20.0 reduce-scatter.7
where the time goes:
time: 279 us; the launch traced here: 278 us
  waiting for transfers between devices  171 us (61%)
  local copies, waits for them, and re-layouts  26.8 us (10%)
  blocking collectives  20.3 us (7%)
  matrix products  18.5 us (7%)
  other arithmetic  15.7 us (6%)
  between operations  14.1 us (5%)
  starting transfers between devices  11.2 us (4%)
    unnamed x5, waiting for transfers between devices  66.2 us
    reduce_scatter x1, waiting for transfers between devices, body(): lax.psum_scatter(gate_terms, 'ep', scatter_dimension=0, tiled=True)  49.9 us
    psum x1, waiting for transfers between devices, body(): lax.psum(partial_mix.astype(jnp.float32).astype(jnp.bfloat16), 'tp')  30.9 us
    all_to_all x1, blocking collectives, body(): lax.all_to_all(hidden_in, 'ep', split_axis=1, concat_axis=0, tiled=True)  14.4 us
    reduce_scatter x1, waiting for transfers between devices, body(): lax.psum_scatter(down_terms.astype(jnp.float32).astype(jnp.bfloat16), 'tp...  12.5 us
    unnamed x40, local copies, waits for them, and re-layouts  8.86 us
    all_to_all x1, waiting for transfers between devices, body(): lax.all_to_all(expert_share, 'ep', split_axis=1, concat_axis=0, tiled=True)  7.32 us
    add x1, other arithmetic, mlstm_step(): keep_old[..., None, None] * memory  6.88 us
  transfers between devices with their start and end apart: 6, of which 6 were waited for; matrix products, arithmetic and copies ran while one was open for 10% of the time, Pallas kernels for 0%

commit v1 on v0

v1 whole, which is shorter than its diff:
```python
import jax
import jax.numpy as jnp
from jax import lax
from jax.experimental import pallas as pl
from jax.experimental.pallas import tpu as pltpu
from jax.sharding import PartitionSpec as P

D = 4096
DH = 128
GROUP_SIZE = 4


res_alpha = 8.0**0.25


def layer_norm(values, gain):
    row_mean = jnp.mean(values, -1, keepdims=True)
    row_var = jnp.mean(values * values, -1, keepdims=True) - row_mean * row_mean
    return (values - row_mean) * lax.rsqrt(row_var + 1e-05) * gain


def cell_kernel(
    input_bias_ref,
    forget_bias_ref,
    parts_ref,
    max_ref,
    gain_ref,
    memory_ref,
    mixed_ref,
    memory_out_ref,
    max_out_ref,
    query_s,
    key_s,
    value_s,
    gate_s,
    keep_s,
    write_s,
    mixed_s,
):
    step = pl.program_id(0)
    heads_here = memory_ref.shape[1]
    head_width = heads_here * DH
    rows = query_s.shape[0]

    @pl.when(step == 0)
    def prepare():
        total = parts_ref[0].astype(jnp.float32)
        for part in range(1, parts_ref.shape[0]):
            total = total + parts_ref[part].astype(jnp.float32)
        gates = total[:, 4 * head_width :]
        gated = gain_ref[...] * jax.nn.sigmoid(total[:, 3 * head_width : 4 * head_width])
        wide = (rows, DH)
        for h in range(heads_here):
            at = h * DH
            query_s[:, h : h + 1, :] = total[:, at : at + DH][:, None, :]
            key_s[:, h : h + 1, :] = (
                total[:, head_width + at : head_width + at + DH] * DH ** (-0.5)
            )[:, None, :]
            value_s[:, h : h + 1, :] = total[:, 2 * head_width + at : 2 * head_width + at + DH][
                :, None, :
            ]
            gate_s[:, h : h + 1, :] = gated[:, at : at + DH][:, None, :]
            f = heads_here + h
            low = 2 * heads_here
            input_sum = gates[:, h : h + 1] + gates[:, low + h : low + h + 1]
            forget_sum = gates[:, f : f + 1] + gates[:, low + f : low + f + 1]
            log_input = jnp.broadcast_to(input_sum, wide) + input_bias_ref[h]
            forget_pre = jnp.broadcast_to(forget_sum, wide) + forget_bias_ref[h]
            log_forget = jnp.minimum(forget_pre, 0.0) - jnp.log1p(jnp.exp(-jnp.abs(forget_pre)))
            carried = log_forget + jnp.broadcast_to(max_ref[:, h : h + 1], wide)
            new_max = jnp.maximum(carried, log_input)
            keep_s[:, h : h + 1, :] = jnp.exp(carried - new_max)[:, None, :]
            write_s[:, h : h + 1, :] = jnp.exp(log_input - new_max)[:, None, :]
            max_out_ref[:, h : h + 1] = new_max[:, 0:1]

    block = memory_ref.shape[0]
    for inner in range(block):
        row = step * block + inner
        query = query_s[row]
        key = key_s[row]
        value = value_s[row]
        keep = keep_s[row]
        write = write_s[row]
        write_key = write * key
        sums = [jnp.zeros_like(query) for _ in range(4)]
        for d in range(DH):
            old = memory_ref[inner, :, d * DH : (d + 1) * DH]
            sums[d % 4] = sums[d % 4] + query[:, d : d + 1] * old
            memory_out_ref[inner, :, d * DH : (d + 1) * DH] = (
                keep * old + write_key[:, d : d + 1] * value
            )
        read_old = (sums[0] + sums[1]) + (sums[2] + sums[3])
        scores = jnp.sum(query * key, -1, keepdims=True) * write
        readout = scores * value + keep * read_old
        scaled = readout * lax.rsqrt(jnp.mean(readout * readout, -1, keepdims=True) + 1e-06)
        mixed_s[row] = scaled * gate_s[row]

    @pl.when(step == pl.num_programs(0) - 1)
    def finish():
        for h in range(heads_here):
            mixed_ref[:, h * DH : (h + 1) * DH] = mixed_s[:, h, :].astype(jnp.bfloat16)


def cell(parts, input_bias, forget_bias, mem_state, max_state, head_gain):
    rows, heads_here, square = mem_state.shape
    head_width = heads_here * DH
    block = 2 if rows % 2 == 0 else 1
    fixed = lambda shape: pl.BlockSpec(shape, lambda i: (0,) * len(shape))
    moving = pl.BlockSpec((block, heads_here, square), lambda i: (i, 0, 0))
    scratch = pltpu.VMEM((rows, heads_here, DH), jnp.float32)
    return pl.pallas_call(
        cell_kernel,
        grid=(rows // block,),
        in_specs=[
            pl.BlockSpec(memory_space=pltpu.SMEM),
            pl.BlockSpec(memory_space=pltpu.SMEM),
            fixed(parts.shape),
            fixed(max_state.shape),
            fixed((1, head_width)),
            moving,
        ],
        out_specs=[fixed((rows, head_width)), moving, fixed(max_state.shape)],
        out_shape=[
            jax.ShapeDtypeStruct((rows, head_width), jnp.bfloat16),
            jax.ShapeDtypeStruct(mem_state.shape, jnp.float32),
            jax.ShapeDtypeStruct(max_state.shape, jnp.float32),
        ],
        scratch_shapes=[scratch] * 7,
        compiler_params=pltpu.CompilerParams(
            dimension_semantics=("arbitrary",), vmem_limit_bytes=16 * 1024 * 1024
        ),
        name="cell",
    )(input_bias, forget_bias, parts, max_state, head_gain.reshape(1, -1), mem_state)


def exchange(blocks, axes):
    return lax.all_to_all(blocks, axes, split_axis=0, concat_axis=0, tiled=True)


def route_weights(mid_float, w_group_router, w_expert_router, expert_route):
    group_logits = jnp.dot(
        mid_float, w_group_router.astype(jnp.float32), precision=lax.Precision.HIGHEST
    )
    expert_logits = jnp.dot(
        mid_float, w_expert_router.astype(jnp.float32), precision=lax.Precision.HIGHEST
    )
    first_expert = expert_route[:, 0]
    second_expert = expert_route[:, 1]
    expert_ids = lax.broadcasted_iota(jnp.int32, expert_logits.shape, 1)
    group_ids = lax.broadcasted_iota(jnp.int32, group_logits.shape, 1)
    first_logit = jnp.sum(jnp.where(expert_ids == first_expert[:, None], expert_logits, 0.0), -1)
    second_logit = jnp.sum(jnp.where(expert_ids == second_expert[:, None], expert_logits, 0.0), -1)
    group_pick = jnp.sum(
        jnp.where(group_ids == (first_expert // GROUP_SIZE)[:, None], group_logits, 0.0), -1
    )
    group_gate = jax.nn.sigmoid(group_pick)
    return (
        group_gate * jax.nn.sigmoid(first_logit - second_logit),
        group_gate * jax.nn.sigmoid(second_logit - first_logit),
    )


def slot_ranks(flat_routes, expert_total):
    onehot = (
        flat_routes[:, None]
        == lax.broadcasted_iota(jnp.int32, (flat_routes.shape[0], expert_total), 1)
    ).astype(jnp.int32)
    running = jnp.cumsum(onehot, 0)
    return jnp.sum((running - 1) * onehot, -1)


def body(
    hidden_in,
    w_query,
    w_key,
    w_value,
    w_outgate,
    w_igate,
    w_fgate,
    input_bias,
    forget_bias,
    mem_state,
    max_state,
    head_gain,
    w_output,
    first_gain,
    w_group_router,
    w_expert_router,
    expert_route,
    w_expgate,
    w_expup,
    w_expdown,
    second_gain,
):
    own_rows, width = hidden_in.shape
    heads_here = mem_state.shape[1]
    head_width = heads_here * DH
    top_count = expert_route.shape[1]
    ep_size = lax.axis_size("ep")
    tp_size = lax.axis_size("tp")
    spread_rows = exchange(
        hidden_in.reshape(own_rows, ep_size, width // ep_size).transpose(1, 0, 2), "ep"
    ).reshape(own_rows * ep_size, width // ep_size)
    stacked_w = jnp.concatenate([w_query, w_key, w_value, w_outgate], 1)
    gate_w = jnp.concatenate([w_igate, w_fgate], 1)
    proj_terms = jnp.dot(spread_rows, stacked_w, preferred_element_type=jnp.float32)
    gate_terms = jnp.dot(spread_rows, gate_w, preferred_element_type=jnp.float32)
    gate_high = lax.reduce_precision(gate_terms, 8, 7)
    gate_low = gate_terms - gate_high
    gate_pad = jnp.zeros((own_rows * ep_size, -4 * heads_here % DH), jnp.bfloat16)
    terms = jnp.concatenate(
        [
            proj_terms.astype(jnp.bfloat16),
            gate_high.astype(jnp.bfloat16),
            gate_low.astype(jnp.bfloat16),
            gate_pad,
        ],
        1,
    )
    parts = exchange(terms.reshape(ep_size, own_rows, terms.shape[1]), "ep")
    mixed_heads, memory_next, new_max = cell(
        parts, input_bias, forget_bias, mem_state, max_state, head_gain
    )
    partial_mix = jnp.dot(mixed_heads, w_output, preferred_element_type=jnp.float32).astype(
        jnp.bfloat16
    )
    mix = jnp.sum(lax.all_gather(partial_mix, "tp").astype(jnp.float32), 0)
    mid_float = layer_norm(res_alpha * hidden_in.astype(jnp.float32) + mix, first_gain)
    mid = mid_float.astype(jnp.bfloat16)
    first_weight, second_weight = route_weights(
        mid_float, w_group_router, w_expert_router, expert_route
    )
    expert_total = w_expgate.shape[0] * ep_size
    capacity = 2 * own_rows * top_count // expert_total
    flat_routes = expert_route.reshape(-1)
    local_slot = flat_routes * capacity + slot_ranks(flat_routes, expert_total)
    share_width = width // tp_size
    mid_share = lax.dynamic_slice_in_dim(mid, lax.axis_index("tp") * share_width, share_width, 1)
    slots = lax.broadcasted_iota(jnp.int32, (expert_total * capacity, own_rows), 0)
    slot_of = local_slot.reshape(own_rows, top_count)
    picks = slots == slot_of[:, 0][None, :]
    for choice in range(1, top_count):
        picks = picks | (slots == slot_of[:, choice][None, :])
    buffer = jnp.dot(picks.astype(jnp.bfloat16), mid, preferred_element_type=jnp.float32).astype(
        jnp.bfloat16
    )
    experts_here = w_expgate.shape[0]
    arrived = (
        exchange(buffer.reshape(ep_size, experts_here * capacity, width), "ep")
        .reshape(ep_size, experts_here, capacity, width)
        .transpose(1, 0, 2, 3)
        .reshape(experts_here, ep_size * capacity, width)
    )
    gate_pre = jnp.einsum("erd,edf->erf", arrived, w_expgate, preferred_element_type=jnp.float32)
    up_pre = jnp.einsum("erd,edf->erf", arrived, w_expup, preferred_element_type=jnp.float32)
    hidden_units = (jax.nn.silu(gate_pre) * up_pre).astype(jnp.bfloat16)
    down_terms = jnp.einsum(
        "erf,efd->erd", hidden_units, w_expdown, preferred_element_type=jnp.float32
    ).astype(jnp.bfloat16)
    outgoing = (
        down_terms.reshape(experts_here, ep_size, capacity, tp_size, share_width)
        .transpose(1, 3, 0, 2, 4)
        .reshape(ep_size * tp_size, experts_here * capacity, share_width)
    )
    returned = exchange(outgoing, ("ep", "tp")).reshape(
        ep_size, tp_size, experts_here * capacity, share_width
    )
    expert_out = (
        jnp.sum(returned.astype(jnp.float32), 1)
        .astype(jnp.bfloat16)
        .reshape(expert_total * capacity, share_width)
    )
    chosen = local_slot[None, :] == lax.broadcasted_iota(
        jnp.int32, (expert_total * capacity, own_rows * top_count), 0
    )
    picked = lax.dot_general(
        chosen.astype(jnp.bfloat16),
        expert_out,
        (((0,), (0,)), ((), ())),
        preferred_element_type=jnp.float32,
    )
    picked = picked.reshape(own_rows, top_count, share_width)
    moe = first_weight[:, None] * picked[:, 0] + second_weight[:, None] * picked[:, 1]
    joined = res_alpha * mid_share.astype(jnp.float32) + moe
    sums = jnp.stack([jnp.sum(joined, -1), jnp.sum(joined * joined, -1)])
    row_sum, square_sum = jnp.sum(lax.all_gather(sums, "tp"), 0)
    row_mean = row_sum / D
    row_var = square_sum / D - row_mean * row_mean
    hidden_out = (
        (joined - row_mean[:, None]) * lax.rsqrt(row_var[:, None] + 1e-05) * second_gain
    ).astype(jnp.bfloat16)
    return (hidden_out, memory_next, new_max)


def solution(mesh):
    return jax.shard_map(
        body,
        mesh=mesh,
        in_specs=(
            P("ep", None),
            P("ep", "tp"),
            P("ep", "tp"),
            P("ep", "tp"),
            P("ep", "tp"),
            P("ep", "tp"),
            P("ep", "tp"),
            P("tp"),
            P("tp"),
            P("ep", "tp", None),
            P("ep", "tp"),
            P("tp"),
            P("tp", None),
            P(),
            P(),
            P(),
            P("ep", None),
            P("ep", None, "tp"),
            P("ep", None, "tp"),
            P("ep", "tp", None),
            P("tp"),
        ),
        out_specs=(P("ep", "tp"), P("ep", "tp", None), P("ep", "tp")),
        check_vma=False,
    )
```

time: 279 us -> 109 us (0.39)
  waiting for transfers between devices: 171 us -> 34.6 us
  local copies, waits for them, and re-layouts: 26.8 us -> 6.28 us
  other arithmetic: 15.7 us -> 2.08 us
  between operations: 14.1 us -> 0.88 us
  blocking collectives: 20.3 us -> 30.9 us
  Pallas kernels: 0 us -> 10.5 us
  matrix products: 18.5 us -> 9.27 us
    unnamed x5 -> x0, waiting for transfers between devices: 66.2 us -> none
    reduce_scatter x2 -> x0, waiting for transfers between devices: 62.4 us -> none  [the longest x1 49.9 us: body(): lax.psum_scatter(gate_terms, 'ep', scatter_dimension=0, tiled=True)]
    psum x1 -> x0, waiting for transfers between devices: 30.9 us -> none  [body(): lax.psum(partial_mix.astype(jnp.float32).astype(jnp.bfloat16), 'tp')]
    all_to_all x2 -> x3, waiting for transfers between devices: 11.8 us -> 34.6 us  [exchange(): return lax.all_to_all(blocks, axes, split_axis=0, concat_axis=0, tiled=True)]
    all_gather x0 -> x2, blocking collectives: none -> 12.4 us  [the longest x1 7.33 us: body(): mix = jnp.sum(lax.all_gather(partial_mix, 'tp').astype(jnp.float32), 0)]
    pallas_call x0 -> x1, Pallas kernels: none -> 10.5 us  [cell(): pl.pallas_call(cell_kernel, grid=(rows // block,), in_specs=[pl.BlockSpec...]
    add x1, other arithmetic: 6.88 us -> 0.01 us  [body(): local_slot = flat_routes * capacity + slot_ranks(flat_routes, expert_total)]
    reshape x2 -> x1, local copies, waits for them, and re-layouts: 6.19 us -> 0.09 us  [body(): flat_routes = expert_route.reshape(-1)]
  transfers between devices with their start and end apart: 6 -> 3, of which waited for: 6 -> 3; matrix products, arithmetic and copies ran while one was open for 10% -> 2% of each run, Pallas kernels for 0% -> 0%
where the time goes in v1:
time: 109 us; the launch traced here: 108 us
  waiting for transfers between devices  34.6 us (32%)
  blocking collectives  30.9 us (28%)
  starting transfers between devices  13.8 us (13%)
  Pallas kernels  10.5 us (10%)
  matrix products  9.27 us (9%)
  local copies, waits for them, and re-layouts  6.28 us (6%)
  other arithmetic  2.08 us (2%)
    all_to_all x3, waiting for transfers between devices, exchange(): return lax.all_to_all(blocks, axes, split_axis=0, concat_axis=0, tiled=True)  34.6 us
    all_to_all x1, blocking collectives, exchange(): return lax.all_to_all(blocks, axes, split_axis=0, concat_axis=0, tiled=True)  18.5 us
    all_to_all x3, starting transfers between devices, exchange(): return lax.all_to_all(blocks, axes, split_axis=0, concat_axis=0, tiled=True)  13.8 us
    pallas_call x1, Pallas kernels, cell(): pl.pallas_call(cell_kernel, grid=(rows // block,), in_specs=[pl.BlockSpec...  10.5 us
    all_gather x1, blocking collectives, body(): mix = jnp.sum(lax.all_gather(partial_mix, 'tp').astype(jnp.float32), 0)  7.33 us
    all_gather x1, blocking collectives, body(): row_sum, square_sum = jnp.sum(lax.all_gather(sums, 'tp'), 0)  5.07 us
    unnamed x32, local copies, waits for them, and re-layouts  4.17 us
    dot_general x1, matrix products, body(): jnp.einsum('erf,efd->erd', hidden_units, w_expdown, preferred_element_typ...  3.82 us
  transfers between devices with their start and end apart: 3, of which 3 were waited for; matrix products, arithmetic and copies ran while one was open for 2% of the time, Pallas kernels for 0%

profile of v1, /device:TPU:0, one launch (start us, length us, event | category | flops | bytes accessed | tf_op | source)
XLA Modules:
  0.0 108.2 jit_solution(16353489706320179273)
XLA Ops:
  0.6 1.1 %copy.60 = bf16[2,8,8,512]{3,2,1,0:T(8,128)(2,1)S(1)} copy(bf16[2,8,8,512]{3,1,2,0:T(8,128)(2,1)} %bitcast.100) | data formatting | bytes 262144
  1.7 0.7 copy.54
  2.4 7.3 %all-to-all-start = ((bf16[8,16,512]{2,1,0:T(8,128)(2,1)}), bf16[8,16,512]{2,1,0:T(8,128)(2,1)S(1)}, u32[]{:S(2)}, u32[]{:S(2)}) async-start(bf16[8,16,512]{2,1,0:T(8,128)(2,1)} %copy.54), calls=%async_computation | async-start | bytes 262144 | tf_op jit(solution)/shard_map/all_to_all | solution.py:137
  9.8 7.3 %all-to-all-done = bf16[8,16,512]{2,1,0:T(8,128)(2,1)S(1)} async-done(((bf16[8,16,512]{2,1,0:T(8,128)(2,1)}), bf16[8,16,512]{2,1,0:T(8,128)(2,1)S(1)}, u32[]{:S(2)}, u32[]{:S(2)}) %all-to-all-start) | async-done | bytes 131104 | tf_op jit(solution)/shard_map/all_to_all | solution.py:137
  17.1 0.8 reduce-precision_convert_fusion
  17.9 2.3 %fusion.1 = bf16[128,2048]{0,1:T(8,128)(2,1)S(1)} fusion(bf16[128,512]{1,0:T(8,128)(2,1)S(1)} %bitcast.102, bf16[512,512]{1,0:T(8,128)(2,1)} %param.25, bf16[512,512]{1,0:T(8,128)(2,1)} %param.24, bf16[512,512]{1,0:T(8,128)(2,1)} %param.23, bf16[512,512]{1,0:T(8,128)(2,1)} %param.22), kind=kOutput, calls=%fused_computation.5 | convolution fusion | flops 277086208 | bytes 2752512 | tf_op jit(solution)/shard_map/dot_general | solution.py:206
  20.3 0.4 maximum_maximum_fusion
  20.6 1.1 copy.55
  21.7 3.5 %all-to-all-start.1 = ((bf16[8,16,2176]{2,1,0:T(8,128)(2,1)}), bf16[8,16,2176]{2,1,0:T(8,128)(2,1)S(1)}, u32[]{:S(2)}, u32[]{:S(2)}) async-start(bf16[8,16,2176]{2,1,0:T(8,128)(2,1)} %bitcast.4), calls=%async_computation.1 | async-start | bytes 1114112 | tf_op jit(solution)/shard_map/all_to_all | solution.py:137
  25.4 0.1 reshape.172
  25.6 0.2 select_reduce_fusion
  25.9 0.1 copy.58
  26.0 13.2 %all-to-all-done.1.parts_ref = bf16[8,16,2176]{2,1,0:T(8,128)(2,1)S(1)} async-done(((bf16[8,16,2176]{2,1,0:T(8,128)(2,1)}), bf16[8,16,2176]{2,1,0:T(8,128)(2,1)S(1)}, u32[]{:S(2)}, u32[]{:S(2)}) %all-to-all-start.1) | async-done | bytes 557088 | tf_op jit(solution)/shard_map/all_to_all | solution.py:137
  39.2 2.2 %copy-done.1 = f32[16,4,16384]{2,1,0:T(4,128)S(1)} copy-done((f32[16,4,16384]{2,1,0:T(4,128)S(1)}, f32[16,4,16384]{2,1,0:T(4,128)}, u32[]{:S(2)}) %copy-start.1) | copy-done | bytes 4194328
  41.4 10.5 %cell.1 = (bf16[16,512]{1,0:T(8,128)(2,1)S(1)}, f32[16,4,16384]{2,1,0:T(4,128)}, f32[16,4]{1,0:T(8,128)S(1)}) custom-call(f32[4]{0:T(128)S(1)} %copy-done.3, f32[4]{0:T(128)S(1)} %copy-done.4, bf16[8,16,2176]{2,1,0:T(8,128)(2,1)S(1)} %all-to-all-done.1.parts_ref, f32[16,4]{1,0:T(8,128)S(1)} %copy.56.max_ref, f32[1,512]{1,0:T(1,128)S(1)} %bitcast.98, ...), custom_call_target="tpu_custom_call" | custom-call | tf_op jit(solution)/shard_map/cell/pallas_call | solution.py:111
  51.9 0.7 convolution_convert_fusion.2
  52.5 7.3 %all-gather = bf16[64,4096]{1,0:T(8,128)(2,1)S(1)} all-gather(bf16[16,4096]{1,0:T(8,128)(2,1)S(1)} %convolution_convert_fusion.2), channel_id=2, replica_groups=mesh['ep'=8,'tp'=4] {'tp'}, dimensions={0}, use_global_device_ids=true | all-gather | bytes 655360 | tf_op jit(solution)/shard_map/all_gather | solution.py:227
  60.0 0.2 fusion.64
  60.2 0.1 fusion.27
  60.3 0.3 fusion
  60.5 18.5 %all_to_all.20 = bf16[8,8,4096]{2,1,0:T(8,128)(2,1)S(1)} all-to-all(bf16[8,8,4096]{2,1,0:T(8,128)(2,1)S(1)} %fusion), channel_id=1, replica_groups=mesh['ep'=8,'tp'=4] {'ep'}, dimensions={0} | all-to-all | bytes 1048576 | tf_op jit(solution)/shard_map/all_to_all | solution.py:137
  79.0 0.5 fusion.12
  79.5 3.8 %convolution_convert_fusion.1 = bf16[64,4096]{1,0:T(8,128)(2,1)} fusion(bf16[1,256,4096]{2,1,0:T(8,128)(2,1)S(1)} %copy-done, bf16[1,4096,256]{2,1,0:T(8,128)(2,1)} %param.39, bf16[8,8,4096]{2,1,0:T(8,128)(2,1)S(1)} %all_to_all.20, f32[64,256]{1,0:T(8,128)S(1)} %fusion.12), kind=kOutput, calls=%fused_computation.1 | convolution fusion | flops 268795904 | bytes 5308416 | tf_op jit(solution)/shard_map/erf,efd->erd/dot_general | solution.py:257
  83.3 3.0 %all-to-all-start.3 = ((bf16[32,8,1024]{2,1,0:T(8,128)(2,1)}), bf16[32,8,1024]{2,1,0:T(8,128)(2,1)S(1)}, u32[]{:S(2)}, u32[]{:S(2)}) async-start(bf16[32,8,1024]{2,1,0:T(8,128)(2,1)} %bitcast.20), calls=%async_computation.3 | async-start | bytes 1048576 | tf_op jit(solution)/shard_map/all_to_all | solution.py:137
  86.3 0.7 copy.59
  87.0 0.4 fusion.22
  87.4 0.4 select_reduce_fusion.2
  87.8 14.1 %all-to-all-done.3 = bf16[32,8,1024]{2,1,0:T(8,128)(2,1)S(1)} async-done(((bf16[32,8,1024]{2,1,0:T(8,128)(2,1)}), bf16[32,8,1024]{2,1,0:T(8,128)(2,1)S(1)}, u32[]{:S(2)}, u32[]{:S(2)}) %all-to-all-start.3) | async-done | bytes 524320 | tf_op jit(solution)/shard_map/all_to_all | solution.py:137
  102.0 0.2 fusion.28
  102.2 0.2 fusion.65
  102.4 5.1 %all-gather.2 = f32[4,2,16]{2,1,0:T(2,128)S(1)} all-gather(f32[1,2,16]{2,1,0:T(2,128)S(1)} %maximum_bitcast_fusion), channel_id=3, replica_groups=mesh['ep'=8,'tp'=4] {'tp'}, dimensions={0}, use_global_device_ids=true | all-gather | bytes 640 | tf_op jit(solution)/shard_map/all_gather | solution.py:286
  107.6 0.7 multiply_convert_fusion
  (46 shorter events, 0.8 us)
Async XLA Ops:
  0.6 78.9 %copy-start = (bf16[1,256,4096]{2,1,0:T(8,128)(2,1)S(1)}, bf16[1,256,4096]{2,1,0:T(8,128)(2,1)}, u32[]{:S(2)}) copy-start(bf16[1,256,4096]{2,1,0:T(8,128)(2,1)} %param.40) | copy-start | bytes 6291460
  2.4 14.6 %all-to-all-start = ((bf16[8,16,512]{2,1,0:T(8,128)(2,1)}), bf16[8,16,512]{2,1,0:T(8,128)(2,1)S(1)}, u32[]{:S(2)}, u32[]{:S(2)}) async-start(bf16[8,16,512]{2,1,0:T(8,128)(2,1)} %copy.54), calls=%async_computation | async-start | bytes 262144 | tf_op jit(solution)/shard_map/all_to_all | solution.py:137
  20.2 5.0 %copy-start.12 = (f32[16,4]{0,1:T(4,128)S(1)}, f32[16,4]{0,1:T(4,128)}, u32[]{:S(2)}) copy-start(f32[16,4]{0,1:T(4,128)} %param.31) | copy-start | bytes 772
  20.2 5.1 %copy-start.10 = (s32[16,2]{0,1:T(2,128)S(1)}, s32[16,2]{0,1:T(2,128)}, u32[]{:S(2)}) copy-start(s32[16,2]{0,1:T(2,128)} %param.37) | copy-start | bytes 388
  20.2 19.0 %copy-start.2 = (f32[512]{0:T(512)S(1)}, f32[512]{0:T(512)}, u32[]{:S(2)}) copy-start(f32[512]{0:T(512)} %param.32) | copy-start | bytes 6148
  20.2 19.0 %copy-start.3 = (f32[4]{0:T(128)S(1)}, f32[4]{0:T(128)}, u32[]{:S(2)}) copy-start(f32[4]{0:T(128)} %input_bias_ref.1) | copy-start | bytes 52
  20.2 18.9 %copy-start.4 = (f32[4]{0:T(128)S(1)}, f32[4]{0:T(128)}, u32[]{:S(2)}) copy-start(f32[4]{0:T(128)} %forget_bias_ref.1) | copy-start | bytes 52
  21.7 17.5 %all-to-all-start.1 = ((bf16[8,16,2176]{2,1,0:T(8,128)(2,1)}), bf16[8,16,2176]{2,1,0:T(8,128)(2,1)S(1)}, u32[]{:S(2)}, u32[]{:S(2)}) async-start(bf16[8,16,2176]{2,1,0:T(8,128)(2,1)} %bitcast.4), calls=%async_computation.1 | async-start | bytes 1114112 | tf_op jit(solution)/shard_map/all_to_all | solution.py:137
  39.2 2.2 %copy-start.1 = (f32[16,4,16384]{2,1,0:T(4,128)S(1)}, f32[16,4,16384]{2,1,0:T(4,128)}, u32[]{:S(2)}) copy-start(f32[16,4,16384]{2,1,0:T(4,128)} %memory_ref.1) | copy-start | bytes 12582916
  41.4 10.5 %copy-start.5 = (bf16[512,4096]{1,0:T(8,128)(2,1)S(1)}, bf16[512,4096]{1,0:T(8,128)(2,1)}, u32[]{:S(2)}) copy-start(bf16[512,4096]{1,0:T(8,128)(2,1)} %param.33) | copy-start | bytes 12582916
  51.9 8.1 %copy-start.7 = (bf16[16,4096]{1,0:T(8,128)(2,1)S(1)}, bf16[16,4096]{1,0:T(8,128)(2,1)}, u32[]{:S(2)}) copy-start(bf16[16,4096]{1,0:T(8,128)(2,1)} %param.21) | copy-start | bytes 393220
  51.9 8.3 %copy-start.9 = (f32[4096]{0:T(1024)S(1)}, f32[4096]{0:T(1024)}, u32[]{:S(2)}) copy-start(f32[4096]{0:T(1024)} %param.34) | copy-start | bytes 49156
  52.5 26.5 %copy-start.6 = (bf16[1,4096,256]{2,1,0:T(8,128)(2,1)S(1)}, bf16[1,4096,256]{2,1,0:T(8,128)(2,1)}, u32[]{:S(2)}) copy-start(bf16[1,4096,256]{2,1,0:T(8,128)(2,1)} %param.38) | copy-start | bytes 6291460
  79.5 7.5 %copy-start.13 = (bf16[4096,2]{0,1:T(2,128)(2,1)S(1)}, bf16[4096,2]{0,1:T(2,128)(2,1)}, u32[]{:S(2)}) copy-start(bf16[4096,2]{0,1:T(2,128)(2,1)} %param.35) | copy-start | bytes 49156
  79.5 7.9 %copy-start.8 = (bf16[4096,8]{0,1:T(8,128)(2,1)S(1)}, bf16[4096,8]{0,1:T(8,128)(2,1)}, u32[]{:S(2)}) copy-start(bf16[4096,8]{0,1:T(8,128)(2,1)} %param.36) | copy-start | bytes 196612
  83.3 24.2 %copy-start.11 = (f32[1024]{0:T(1024)S(1)}, f32[1024]{0:T(1024)}, u32[]{:S(2)}) copy-start(f32[1024]{0:T(1024)} %param.41) | copy-start | bytes 12292
  83.3 18.6 %all-to-all-start.3 = ((bf16[32,8,1024]{2,1,0:T(8,128)(2,1)}), bf16[32,8,1024]{2,1,0:T(8,128)(2,1)S(1)}, u32[]{:S(2)}, u32[]{:S(2)}) async-start(bf16[32,8,1024]{2,1,0:T(8,128)(2,1)} %bitcast.20), calls=%async_computation.3 | async-start | bytes 1048576 | tf_op jit(solution)/shard_map/all_to_all | solution.py:137
